TPU v7x, 32 devices: a whole 2x2x4 slice. The times are simulated.
32 devices in a mesh: sp: 8 (over z, y), tp: 4 (over x, core).
Axes of the slice: x: 2, y: 2, z: 4, core: 2. Of those that a mesh axis runs over, the one named last changes fastest.
Arguments:
- tokens: bfloat16 [4096, 2048], P(('sp', 'tp')), may hold values from -6 to 6
- queries: bfloat16 [4096, 1024], P('sp', 'tp'), may hold values from -160 to 160
- keys: bfloat16 [4096, 1024], P('sp', 'tp'), may hold values from -8 to 8
- values: bfloat16 [4096, 1024], P('sp', 'tp'), may hold values from -6 to 6
- lambdas: float32 [8], P('tp'), may hold values from 0.3 to 0.8
- head_gain: float32 [128], replicated, may hold values from 0.1 to 1.9
- out_weight: bfloat16 [1024, 2048], replicated, may hold values from -0.1875 to 0.1875
- mixer_gain: float32 [2048], replicated, may hold values from 0.1 to 1.9
- up_weight: bfloat16 [2048, 4096], P('sp', 'tp'), may hold values from -0.125 to 0.125
- down_weight: bfloat16 [4096, 2048], P('tp', 'sp'), may hold values from -0.09375 to 0.09375
Outputs:
- result: bfloat16 [4096, 2048], P(('sp', 'tp'))
All inputs are finite; a program needn't handle non-finite values.
Results may differ from a plain program's by a relative error of at most 0.02.
Values may be sent and summed in bfloat16 or wider, within the bound.
A program may use at most 128 MiB of HBM per device.

v0:
```python
import math
import jax
import jax.numpy as jnp
from jax import lax
from jax.sharding import PartitionSpec as P

DQK = 64
DV = 128


def per_device(
    tokens,
    queries,
    keys,
    values,
    lambdas,
    head_gain,
    out_weight,
    mixer_gain,
    up_weight,
    down_weight,
):
    tok_rows = queries.shape[0]
    head_count = lambdas.shape[0]
    scaling = DQK ** (-0.5)
    sp_index = lax.axis_index("sp")
    first_row = sp_index * tok_rows
    last_row = first_row + tok_rows - 1
    query_split = queries.reshape(tok_rows, head_count, 2, DQK)
    query_pos = first_row + lax.broadcasted_iota(jnp.int32, (tok_rows, 1), 0)
    floor_max = jnp.full((head_count, tok_rows), -1e30, jnp.float32)
    zero_total = jnp.zeros((head_count, tok_rows), jnp.float32)
    zero_acc = jnp.zeros((head_count, tok_rows, DV), jnp.float32)
    start_state = (floor_max, zero_total, zero_acc, floor_max, zero_total, zero_acc)
    key_piece = lax.all_gather(keys, "sp", axis=0, tiled=True)
    value_piece = lax.all_gather(values, "sp", axis=0, tiled=True)
    piece_rows = key_piece.shape[0]
    block_width = math.gcd(piece_rows, 512)

    def one_block(block_index, running):
        offset = block_index * block_width

        def update(inner):
            key_block = lax.dynamic_slice_in_dim(key_piece, offset, block_width, 0).reshape(
                block_width, head_count, 2, DQK
            )
            value_block = lax.dynamic_slice_in_dim(value_piece, offset, block_width, 0).reshape(
                block_width, head_count, DV
            )
            key_pos = offset + lax.broadcasted_iota(jnp.int32, (1, block_width), 1)
            allowed = key_pos <= query_pos
            updated = []
            for map_index in range(2):
                run_max = inner[3 * map_index]
                run_total = inner[3 * map_index + 1]
                run_acc = inner[3 * map_index + 2]
                scores = (
                    jnp.einsum(
                        "qhd,khd->hqk",
                        query_split[:, :, map_index],
                        key_block[:, :, map_index],
                        preferred_element_type=jnp.float32,
                    )
                    * scaling
                )
                scores = jnp.where(allowed[None], scores, -jnp.inf)
                new_max = jnp.maximum(run_max, jnp.max(scores, axis=2))
                shrink = jnp.exp(run_max - new_max)
                exponent = jnp.exp(scores - new_max[:, :, None])
                new_total = run_total * shrink + jnp.sum(exponent, axis=2)
                new_acc = run_acc * shrink[:, :, None] + jnp.einsum(
                    "hqk,khd->hqd",
                    exponent.astype(jnp.bfloat16),
                    value_block,
                    preferred_element_type=jnp.float32,
                )
                updated += [new_max, new_total, new_acc]
            return tuple(updated)

        return lax.cond(offset <= last_row, update, lambda inner: inner, running)

    final = lax.fori_loop(0, piece_rows // block_width, one_block, start_state)
    first_map = final[2] / final[1][:, :, None]
    second_map = final[5] / final[4][:, :, None]
    differ = first_map - lambdas[:, None, None] * second_map
    spread = lax.rsqrt(jnp.mean(differ * differ, axis=2, keepdims=True) + 1e-06)
    attended = (differ * spread * head_gain).astype(jnp.bfloat16)
    attended = jnp.transpose(attended, (1, 0, 2)).reshape(tok_rows, head_count * DV)
    all_heads = lax.all_to_all(attended, "tp", split_axis=0, concat_axis=1, tiled=True)
    projected = jnp.dot(all_heads, out_weight, preferred_element_type=jnp.float32).astype(
        jnp.bfloat16
    )
    resid = (tokens.astype(jnp.float32) + projected.astype(jnp.float32)).astype(jnp.bfloat16)
    resid_full = resid.astype(jnp.float32)
    normed = (
        resid_full
        * lax.rsqrt(jnp.mean(resid_full * resid_full, axis=1, keepdims=True) + 1e-06)
        * mixer_gain
    ).astype(jnp.bfloat16)
    up_full, down_full = (
        lax.all_gather(up_weight, "sp", axis=0, tiled=True),
        lax.all_gather(down_weight, "sp", axis=1, tiled=True),
    )
    hidden = jnp.square(
        jax.nn.relu(
            jnp.dot(
                lax.all_gather(normed, "tp", axis=0, tiled=True),
                up_full,
                preferred_element_type=jnp.float32,
            )
        )
    ).astype(jnp.bfloat16)
    mixed = lax.psum_scatter(
        jnp.dot(hidden, down_full, preferred_element_type=jnp.float32).astype(jnp.bfloat16),
        "tp",
        scatter_dimension=0,
        tiled=True,
    ).astype(jnp.float32)
    return (resid_full + mixed).astype(jnp.bfloat16)


def solution(mesh):
    placed = (
        P(("sp", "tp"), None),
        P("sp", "tp"),
        P("sp", "tp"),
        P("sp", "tp"),
        P("tp"),
        P(),
        P(),
        P(),
        P("sp", "tp"),
        P("tp", "sp"),
    )
    return jax.shard_map(
        per_device, mesh=mesh, in_specs=placed, out_specs=P(("sp", "tp"), None), check_vma=False
    )
```

profile of v0, /device:TPU:0, one launch (start us, length us, event | category | flops | bytes accessed | tf_op | source)
XLA Modules:
  0.0 390.4 jit_solution(7003081648482967234)
XLA Ops:
  6.5 0.0 all-gather.6.cloned.1.call-start
  6.5 1.8 copy.19
  8.3 0.0 all-gather.6.cloned.1.call-update
  8.4 0.0 all-gather.8.cloned.1.call-start
  8.4 1.8 copy.21
  10.2 0.0 all-gather.8.cloned.1.call-update
  10.2 0.0 all-gather.10.cloned.1.call-start
  10.3 1.1 copy.20
  11.4 51.1 %all-gather.6.cloned.1.call-done = bf16[4096,256]{0,1:T(8,128)(2,1)} async-done(((bf16[512,256]{0,1:T(8,128)(2,1)}), bf16[4096,256]{0,1:T(8,128)(2,1)}) %all-gather.6.cloned.1.call-update) | async-done | bytes 2097168 | tf_op jit(solution)/shard_map/all_gather | solution.py:35
  62.5 50.6 %all-gather.8.cloned.1.call-done = bf16[4096,256]{0,1:T(8,128)(2,1)} async-done(((bf16[512,256]{0,1:T(8,128)(2,1)}), bf16[4096,256]{0,1:T(8,128)(2,1)}) %all-gather.8.cloned.1.call-update) | async-done | bytes 2097168 | tf_op jit(solution)/shard_map/all_gather | solution.py:36
  113.2 0.0 copy-start.2
  113.2 0.0 copy-start.3
  113.2 6.1 %while.24 = (s32[]{:T(128)}, f32[2,512]{1,0:T(2,128)S(1)}, f32[2,512]{1,0:T(2,128)S(1)}, f32[2,512,128]{2,1,0:T(8,128)S(1)}, f32[2,512]{1,0:T(2,128)S(1)}, /*ind...) while((s32[]{:T(128)}, f32[2,512]{1,0:T(2,128)S(1)}, ...), condition=%wide.region_7.8_spmd.clone, body=%wide.region_0.7_spmd.clone.sunk | while | flops 410784768 | bytes 17707416 | solution.py:82
  113.3 5.6 %conditional.3 = ((f32[2,512]{1,0:T(2,128)S(1)}, f32[2,512]{1,0:T(2,128)S(1)}, f32[2,512,128]{2,1,0:T(8,128)S(1)}, f32[2,512]{1,0:T(2,128)S(1)}, f32[2,512]{1,0:T(2,128)S(1)}, /*index=5*/f32[2,512,128]{2,1,0:T(8,128)S(1)})) conditional(s32[]{:T(128)} %convert_element_type.94, (f32[2,512]{1,0:T(2,128)S(1)}, f32[2,512]{1,0:T(2,128)S(1)}, ...), branch_computations={%region_1.0_spmd, %region_2.6_spmd} | conditional | flops 410784768 | bytes 17705066 | solution.py:80
  113.3 1.0 constant_dynamic-slice_fusion.1
  114.3 0.2 broadcast_compare_fusion
  114.5 0.6 fusion.20
  115.2 0.3 fusion.3
  115.5 0.6 fusion.21
  116.1 0.3 fusion.5
  116.4 1.0 constant_dynamic-slice_fusion
  117.4 0.7 convolution_add_fusion
  118.1 0.7 convolution_add_fusion.1
  119.3 0.0 copy-done.2
  119.3 0.0 copy-start
  119.3 0.5 multiply_reduce_fusion.1
  119.9 0.0 copy-done.3
  119.9 0.2 fusion.18
  120.1 0.3 copy.23
  120.4 0.2 all_to_all.14
  120.5 8.5 %all_to_all.19 = bf16[4,128,256]{2,1,0:T(8,128)(2,1)S(1)} all-to-all(bf16[4,128,256]{2,1,0:T(8,128)(2,1)S(1)} %all_to_all.14), channel_id=1, replica_groups=mesh['sp'=8,'tp'=4] {'tp'}, dimensions={0} | all-to-all | bytes 524288 | tf_op jit(solution)/shard_map/all_to_all | solution.py:89
  129.1 0.2 copy.24
  129.3 0.0 copy-start.1
  129.3 3.0 multiply_reduce_fusion
  132.3 1.0 multiply_convert_fusion.1
  133.3 0.0 all-gather.10.cloned.1.call-update
  133.3 0.0 all-gather.12.cloned.1.call-start
  133.3 0.5 all-gather.12.cloned.1.call-update
  133.9 0.0 all-gather.14.cloned.1.call-start
  133.9 0.5 all-gather.14.cloned.1.call-update
  134.5 0.0 reduce-scatter.2.cloned.1.call-start
  134.5 57.8 %all-gather.10.cloned.1.call-done = bf16[512,2048]{1,0:T(8,128)(2,1)} async-done(((bf16[128,2048]{1,0:T(8,128)(2,1)}), bf16[512,2048]{1,0:T(8,128)(2,1)}) %all-gather.10.cloned.1.call-update) | async-done | bytes 2097168 | tf_op jit(solution)/shard_map/all_gather | solution.py:107
  192.3 74.8 %all-gather.12.cloned.1.call-done = bf16[2048,1024]{1,0:T(8,128)(2,1)} async-done(((bf16[256,1024]{1,0:T(8,128)(2,1)}), bf16[2048,1024]{1,0:T(8,128)(2,1)}) %all-gather.12.cloned.1.call-update) | async-done | bytes 4194320 | tf_op jit(solution)/shard_map/all_gather | solution.py:101
  267.1 75.1 %all-gather.14.cloned.1.call-done = bf16[1024,2048]{1,0:T(8,128)(2,1)} async-done(((bf16[1024,256]{1,0:T(8,128)(2,1)}), bf16[1024,2048]{1,0:T(8,128)(2,1)}) %all-gather.14.cloned.1.call-update) | async-done | bytes 4194320 | tf_op jit(solution)/shard_map/all_gather | solution.py:102
  342.2 9.9 %convolution_convert_fusion = bf16[512,2048]{1,0:T(8,128)(2,1)} fusion(bf16[1024,2048]{1,0:T(8,128)(2,1)} %all-gather.14.cloned.1.call-done, bf16[512,2048]{1,0:T(8,128)(2,1)} %all-gather.10.cloned.1.call-done, bf16[2048,1024]{1,0:T(8,128)(2,1)} %all-gather.12.cloned.1.call-done), kind=kOutput, calls=%fused_computation.28 | convolution fusion | flops 4297588736 | bytes 12582912 | tf_op jit(solution)/shard_map/dot_general | solution.py:114
  352.1 0.0 reduce-scatter.2.cloned.1.call-update
  352.1 29.5 %reduce-scatter.2.cloned.1.call-done = bf16[128,2048]{1,0:T(8,128)(2,1)} async-done(((bf16[512,2048]{1,0:T(8,128)(2,1)}), bf16[128,2048]{1,0:T(8,128)(2,1)}) %reduce-scatter.2.cloned.1.call-update) | async-done | bytes 524304 | tf_op jit(solution)/shard_map/reduce_scatter | solution.py:113
  381.6 1.9 add_convert_fusion
  (33 shorter events, 0.3 us)
Async XLA Ops:
  6.5 55.9 %all-gather.6.cloned.1.call-start = ((), (), s32[]{:S(2)}) async-start(), calls=%async_computation.2 | async-start | bytes 2359296 | tf_op jit(solution)/shard_map/all_gather | solution.py:35
  8.4 104.7 %all-gather.8.cloned.1.call-start = ((), (), s32[]{:S(2)}) async-start(), calls=%async_computation.3 | async-start | bytes 2359296 | tf_op jit(solution)/shard_map/all_gather | solution.py:36
  10.2 182.1 %all-gather.10.cloned.1.call-start = ((), (), s32[]{:S(2)}) async-start(), calls=%async_computation.4 | async-start | bytes 2621440 | tf_op jit(solution)/shard_map/all_gather | solution.py:107
  113.2 6.1 %copy-start.2 = (f32[2]{0:T(128)S(1)}, f32[2]{0:T(128)}, u32[]{:S(2)}) copy-start(f32[2]{0:T(128)} %param.18) | copy-start | bytes 28
  113.2 6.6 %copy-start.3 = (f32[128]{0:T(128)S(1)}, f32[128]{0:T(128)}, u32[]{:S(2)}) copy-start(f32[128]{0:T(128)} %param.19) | copy-start | bytes 1540
  119.3 9.9 %copy-start = (bf16[128,2048]{1,0:T(8,128)(2,1)S(1)}, bf16[128,2048]{1,0:T(8,128)(2,1)}, u32[]{:S(2)}) copy-start(bf16[128,2048]{1,0:T(8,128)(2,1)} %param.14) | copy-start | bytes 1572868
  129.3 3.0 copy-start.1
  133.3 133.8 %all-gather.12.cloned.1.call-start = ((), (), s32[]{:S(2)}) async-start(), calls=%async_computation.5 | async-start | bytes 4718592 | tf_op jit(solution)/shard_map/all_gather | solution.py:101
  133.9 208.3 %all-gather.14.cloned.1.call-start = ((), (), s32[]{:S(2)}) async-start(), calls=%async_computation.6 | async-start | bytes 4718592 | tf_op jit(solution)/shard_map/all_gather | solution.py:102
  134.5 247.2 %reduce-scatter.2.cloned.1.call-start = ((), (), s32[]{:S(2)}) async-start(), calls=%async_computation.7 | async-start | bytes 2621440 | tf_op jit(solution)/shard_map/reduce_scatter | solution.py:113
Sparse Core Ops, SparseCore 0:
  9.4 53.0 all-gather.5
  64.5 48.5 all-gather.7
  133.4 58.8 all-gather.9
  194.3 72.7 all-gather.11
  269.0 73.1 all-gather.13
  352.3 29.3 reduce-scatter.1
where the time goes:
time: 391 us; the launch traced here: 390 us
  waiting for transfers between devices  340 us (87%)
  matrix products  15.6 us (4%)
  between operations  13.6 us (3%)
  blocking collectives  8.55 us (2%)
  local copies, waits for them, and re-layouts  7.41 us (2%)
  other arithmetic  4.49 us (1%)
    all_gather x1, waiting for transfers between devices, per_device(): lax.all_gather(down_weight, 'sp', axis=1, tiled=True)  75.1 us
    all_gather x1, waiting for transfers between devices, per_device(): lax.all_gather(up_weight, 'sp', axis=0, tiled=True)  74.8 us
    all_gather x1, waiting for transfers between devices, per_device(): lax.all_gather(normed, 'tp', axis=0, tiled=True)  57.8 us
    all_gather x1, waiting for transfers between devices, per_device(): key_piece = lax.all_gather(keys, 'sp', axis=0, tiled=True)  51.1 us
    all_gather x1, waiting for transfers between devices, per_device(): value_piece = lax.all_gather(values, 'sp', axis=0, tiled=True)  50.6 us
    reduce_scatter x1, waiting for transfers between devices, per_device(): lax.psum_scatter(jnp.dot(hidden, down_full, preferred_element_type=jnp.fl...  29.5 us
    dot_general x1, matrix products, per_device(): jnp.dot(hidden, down_full, preferred_element_type=jnp.float32)  9.93 us
    all_to_all x1, blocking collectives, per_device(): lax.all_to_all(attended, 'tp', split_axis=0, concat_axis=1, tiled=True)  8.55 us
  transfers between devices with their start and end apart: 6, of which 6 were waited for; matrix products, arithmetic and copies ran while one was open for 1% of the time, Pallas kernels for 0%

commit v1 on v0

--- a/solution.py
+++ b/solution.py
@@ -32,8 +32,11 @@
     zero_total = jnp.zeros((head_count, tok_rows), jnp.float32)
     zero_acc = jnp.zeros((head_count, tok_rows, DV), jnp.float32)
     start_state = (floor_max, zero_total, zero_acc, floor_max, zero_total, zero_acc)
-    key_piece = lax.all_gather(keys, "sp", axis=0, tiled=True)
-    value_piece = lax.all_gather(values, "sp", axis=0, tiled=True)
+    key_piece, value_piece = jnp.split(
+        lax.all_gather(jnp.concatenate([keys, values], axis=1), "sp", axis=0, tiled=True),
+        [keys.shape[1]],
+        axis=1,
+    )
     piece_rows = key_piece.shape[0]
     block_width = math.gcd(piece_rows, 512)
 

time: 391 us -> 308 us (0.79)
  waiting for transfers between devices: 340 us -> 256 us
    all_gather x1, waiting for transfers between devices: 57.8 us -> 22.5 us  [per_device(): lax.all_gather(normed, 'tp', axis=0, tiled=True)]
    all_gather x2 -> x1, waiting for transfers between devices: 102 us -> 75.8 us  [per_device(): lax.all_gather(jnp.concatenate([keys, values], axis=1), 'sp', axis=0, til...]
    all_gather x1, waiting for transfers between devices: 75.1 us -> 51.6 us  [per_device(): lax.all_gather(down_weight, 'sp', axis=1, tiled=True)]
    split x0 -> x1, local copies, waits for them, and re-layouts: none -> 3.94 us  [per_device(): jnp.split(lax.all_gather(jnp.concatenate([keys, values], axis=1), 'sp', a...]
  transfers between devices with their start and end apart: 6 -> 5, of which waited for: 6 -> 5; matrix products, arithmetic and copies ran while one was open for 1% -> 5% of each run, Pallas kernels for 0% -> 0%
where the time goes in v1:
time: 308 us; the launch traced here: 307 us
  waiting for transfers between devices  256 us (83%)
  matrix products  15.6 us (5%)
  between operations  13.3 us (4%)
  blocking collectives  8.59 us (3%)
  local copies, waits for them, and re-layouts  8.09 us (3%)
  other arithmetic  5.32 us (2%)
    all_gather x1, waiting for transfers between devices, per_device(): lax.all_gather(jnp.concatenate([keys, values], axis=1), 'sp', axis=0, til...  75.8 us
    all_gather x1, waiting for transfers between devices, per_device(): lax.all_gather(up_weight, 'sp', axis=0, tiled=True)  73.1 us
    all_gather x1, waiting for transfers between devices, per_device(): lax.all_gather(down_weight, 'sp', axis=1, tiled=True)  51.6 us
    reduce_scatter x1, waiting for transfers between devices, per_device(): lax.psum_scatter(jnp.dot(hidden, down_full, preferred_element_type=jnp.fl...  31.3 us
    all_gather x1, waiting for transfers between devices, per_device(): lax.all_gather(normed, 'tp', axis=0, tiled=True)  22.5 us
    dot_general x1, matrix products, per_device(): jnp.dot(hidden, down_full, preferred_element_type=jnp.float32)  9.93 us
    all_to_all x1, blocking collectives, per_device(): lax.all_to_all(attended, 'tp', split_axis=0, concat_axis=1, tiled=True)  8.59 us
  transfers between devices with their start and end apart: 5, of which 5 were waited for; matrix products, arithmetic and copies ran while one was open for 5% of the time, Pallas kernels for 0%

profile of v1, /device:TPU:0, one launch (start us, length us, event | category | flops | bytes accessed | tf_op | source)
XLA Modules:
  0.0 307.5 jit_solution(1780233604180829738)
XLA Ops:
  6.5 0.0 all-gather.5.cloned.1.call-start
  6.5 1.1 copy.19
  7.7 1.1 copy.20
  8.8 0.8 pad_maximum_fusion
  9.6 0.0 all-gather.5.cloned.1.call-update
  9.6 0.0 all-gather.11.cloned.1.call-start
  9.7 0.7 all-gather.11.cloned.1.call-update
  10.4 0.0 all-gather.9.cloned.1.call-start
  10.4 0.7 all-gather.9.cloned.1.call-update
  11.1 0.0 all-gather.7.cloned.1.call-start
  11.2 0.0 copy-done.1
  11.2 0.1 copy.21
  11.4 75.8 %all-gather.5.cloned.1.call-done = bf16[4096,512]{0,1:T(8,128)(2,1)} async-done(((bf16[512,512]{0,1:T(8,128)(2,1)}), bf16[4096,512]{0,1:T(8,128)(2,1)}) %all-gather.5.cloned.1.call-update) | async-done | bytes 4194320 | tf_op jit(solution)/shard_map/all_gather | solution.py:36
  87.1 3.9 %fusion.22 = (bf16[4096,256]{0,1:T(8,128)(2,1)S(1)}, bf16[4096,256]{0,1:T(8,128)(2,1)}) fusion(bf16[4096,512]{0,1:T(8,128)(2,1)} %all-gather.5.cloned.1.call-done), kind=kLoop, calls=%fused_computation.48 | loop fusion | bytes 8388608 | tf_op jit(solution)/shard_map/split | solution.py:35
  91.2 0.0 copy-start.3
  91.2 0.0 copy-start.4
  91.2 5.1 %while.24 = (s32[]{:T(128)}, f32[2,512]{1,0:T(2,128)S(1)}, f32[2,512]{1,0:T(2,128)S(1)}, f32[2,512,128]{2,1,0:T(8,128)S(1)}, f32[2,512]{1,0:T(2,128)S(1)}, /*ind...) while((s32[]{:T(128)}, f32[2,512]{1,0:T(2,128)S(1)}, ...), condition=%wide.region_7.8_spmd.clone, body=%wide.region_0.7_spmd.clone.sunk | while | flops 410784768 | bytes 17707416 | solution.py:85
  91.3 4.6 %conditional.3 = ((f32[2,512]{1,0:T(2,128)S(1)}, f32[2,512]{1,0:T(2,128)S(1)}, f32[2,512,128]{2,1,0:T(8,128)S(1)}, f32[2,512]{1,0:T(2,128)S(1)}, f32[2,512]{1,0:T(2,128)S(1)}, /*index=5*/f32[2,512,128]{2,1,0:T(8,128)S(1)})) conditional(s32[]{:T(128)} %convert_element_type.94, (f32[2,512]{1,0:T(2,128)S(1)}, f32[2,512]{1,0:T(2,128)S(1)}, ...), branch_computations={%region_1.0_spmd, %region_2.6_spmd} | conditional | flops 410784768 | bytes 17705066 | solution.py:83
  91.3 1.0 constant_dynamic-slice_fusion.1
  92.3 0.2 broadcast_compare_fusion
  92.5 0.6 fusion.20
  93.2 0.3 fusion.3
  93.5 0.6 fusion.21
  94.1 0.3 fusion.5
  94.5 0.7 convolution_add_fusion
  95.2 0.7 convolution_add_fusion.1
  96.3 0.0 copy-done.3
  96.4 0.0 copy-start
  96.4 0.5 multiply_reduce_fusion.1
  96.9 0.0 copy-done.4
  96.9 0.2 fusion.18
  97.1 0.3 copy.23
  97.4 0.2 all_to_all.14
  97.6 8.6 %all_to_all.19 = bf16[4,128,256]{2,1,0:T(8,128)(2,1)S(1)} all-to-all(bf16[4,128,256]{2,1,0:T(8,128)(2,1)S(1)} %all_to_all.14), channel_id=1, replica_groups=mesh['sp'=8,'tp'=4] {'tp'}, dimensions={0} | all-to-all | bytes 524288 | tf_op jit(solution)/shard_map/all_to_all | solution.py:92
  106.2 0.2 copy.24
  106.3 0.0 copy-done
  106.3 0.0 copy-start.2
  106.4 3.0 multiply_reduce_fusion
  109.4 1.0 multiply_convert_fusion.1
  110.4 0.0 all-gather.7.cloned.1.call-update
  110.4 0.0 reduce-scatter.2.cloned.1.call-start
  110.4 51.6 %all-gather.11.cloned.1.call-done = bf16[1024,2048]{1,0:T(8,128)(2,1)} async-done(((bf16[1024,256]{1,0:T(8,128)(2,1)}), bf16[1024,2048]{1,0:T(8,128)(2,1)}) %all-gather.11.cloned.1.call-update) | async-done | bytes 4194320 | tf_op jit(solution)/shard_map/all_gather | solution.py:105
  162.0 73.1 %all-gather.9.cloned.1.call-done = bf16[2048,1024]{1,0:T(8,128)(2,1)} async-done(((bf16[256,1024]{1,0:T(8,128)(2,1)}), bf16[2048,1024]{1,0:T(8,128)(2,1)}) %all-gather.9.cloned.1.call-update) | async-done | bytes 4194320 | tf_op jit(solution)/shard_map/all_gather | solution.py:104
  235.2 22.5 %all-gather.7.cloned.1.call-done = bf16[512,2048]{1,0:T(8,128)(2,1)} async-done(((bf16[128,2048]{1,0:T(8,128)(2,1)}), bf16[512,2048]{1,0:T(8,128)(2,1)}) %all-gather.7.cloned.1.call-update) | async-done | bytes 2097168 | tf_op jit(solution)/shard_map/all_gather | solution.py:110
  257.7 9.9 %convolution_convert_fusion = bf16[512,2048]{1,0:T(8,128)(2,1)} fusion(bf16[1024,2048]{1,0:T(8,128)(2,1)} %all-gather.11.cloned.1.call-done, bf16[512,2048]{1,0:T(8,128)(2,1)} %all-gather.7.cloned.1.call-done, bf16[2048,1024]{1,0:T(8,128)(2,1)} %all-gather.9.cloned.1.call-done), kind=kOutput, calls=%fused_computation.28 | convolution fusion | flops 4297588736 | bytes 12582912 | tf_op jit(solution)/shard_map/dot_general | solution.py:117
  267.6 0.0 reduce-scatter.2.cloned.1.call-update
  267.7 31.3 %reduce-scatter.2.cloned.1.call-done = bf16[128,2048]{1,0:T(8,128)(2,1)} async-done(((bf16[512,2048]{1,0:T(8,128)(2,1)}), bf16[128,2048]{1,0:T(8,128)(2,1)}) %reduce-scatter.2.cloned.1.call-update) | async-done | bytes 524304 | tf_op jit(solution)/shard_map/reduce_scatter | solution.py:116
  299.0 1.9 add_convert_fusion
  (34 shorter events, 0.3 us)
Async XLA Ops:
  6.5 4.6 %copy-start.1 = (bf16[512,256]{1,0:T(8,128)(2,1)S(1)}, bf16[512,256]{1,0:T(8,128)(2,1)}, u32[]{:S(2)}) copy-start(bf16[512,256]{1,0:T(8,128)(2,1)} %param.15) | copy-start | bytes 786436
  6.5 80.6 %all-gather.5.cloned.1.call-start = ((), (), s32[]{:S(2)}) async-start(), calls=%async_computation.2 | async-start | bytes 4718592 | tf_op jit(solution)/shard_map/all_gather | solution.py:36
  9.6 152.4 %all-gather.11.cloned.1.call-start = ((), (), s32[]{:S(2)}) async-start(), calls=%async_computation.5 | async-start | bytes 4718592 | tf_op jit(solution)/shard_map/all_gather | solution.py:105
  10.4 224.8 %all-gather.9.cloned.1.call-start = ((), (), s32[]{:S(2)}) async-start(), calls=%async_computation.4 | async-start | bytes 4718592 | tf_op jit(solution)/shard_map/all_gather | solution.py:104
  11.1 246.6 %all-gather.7.cloned.1.call-start = ((), (), s32[]{:S(2)}) async-start(), calls=%async_computation.3 | async-start | bytes 2621440 | tf_op jit(solution)/shard_map/all_gather | solution.py:110
  91.2 5.1 %copy-start.3 = (f32[2]{0:T(128)S(1)}, f32[2]{0:T(128)}, u32[]{:S(2)}) copy-start(f32[2]{0:T(128)} %param.18) | copy-start | bytes 28
  91.2 5.7 %copy-start.4 = (f32[128]{0:T(128)S(1)}, f32[128]{0:T(128)}, u32[]{:S(2)}) copy-start(f32[128]{0:T(128)} %param.19) | copy-start | bytes 1540
  96.4 10.0 %copy-start = (bf16[128,2048]{1,0:T(8,128)(2,1)S(1)}, bf16[128,2048]{1,0:T(8,128)(2,1)}, u32[]{:S(2)}) copy-start(bf16[128,2048]{1,0:T(8,128)(2,1)} %param.14) | copy-start | bytes 1572868
  106.3 3.1 copy-start.2
  110.4 188.6 %reduce-scatter.2.cloned.1.call-start = ((), (), s32[]{:S(2)}) async-start(), calls=%async_computation.6 | async-start | bytes 2621440 | tf_op jit(solution)/shard_map/reduce_scatter | solution.py:116
Sparse Core Ops, SparseCore 0:
  9.8 77.3 all-gather.4
  89.2 72.8 all-gather.10
  164.2 70.9 all-gather.8
  236.6 21.0 all-gather.6
  267.8 31.1 reduce-scatter.1
